TPU v7x, 32 devices: a whole 2x2x4 slice. The times are simulated.
32 devices in a mesh: kv: 8 (over z, x), tp: 4 (over y, core).
Axes of the slice: x: 2, y: 2, z: 4, core: 2. Of those that a mesh axis runs over, the one named last changes fastest.
Arguments:
- stream: bfloat16 [128, 4096], P(None, ('kv', 'tp')), may hold values from -20 to 20
- ssm_state: float32 [128, 64, 64, 128], P('kv', 'tp'), may hold values from -1.8 to 1.8
- conv_state: bfloat16 [128, 3, 8, 768], P('kv', None, 'tp'), may hold values from -6 to 6
- first_gain: float32 [4096], P(('kv', 'tp')), may hold values from 0.1 to 1.9
- first_gate: bfloat16 [4096, 11264], P('kv', 'tp'), may hold values from -0.09375 to 0.09375
- first_up: bfloat16 [4096, 11264], P('kv', 'tp'), may hold values from -0.09375 to 0.09375
- first_down: bfloat16 [11264, 4096], P('tp', 'kv'), may hold values from -0.0546875 to 0.0546875
- mix_gain: float32 [4096], P(('kv', 'tp')), may hold values from 0.1 to 1.9
- gate_in: bfloat16 [4096, 4096], P('kv', 'tp'), may hold values from -0.09375 to 0.09375
- value_in: bfloat16 [4096, 4096], P('kv', 'tp'), may hold values from -0.09375 to 0.09375
- write_in: bfloat16 [4096, 1024], P('kv', 'tp'), may hold values from -0.09375 to 0.09375
- read_in: bfloat16 [4096, 1024], P('kv', 'tp'), may hold values from -0.09375 to 0.09375
- step_in: bfloat16 [4096, 64], P('kv', 'tp'), may hold values from -0.09375 to 0.09375
- conv_weight: float32 [4, 8, 768], P(None, 'tp'), may hold values from -3 to 3
- step_bias: float32 [64], P('tp'), may hold values from -3 to 0.5
- log_decay_rate: float32 [64], P('tp'), may hold values from -1 to 2.5
- group_gain: float32 [4096], P('tp'), may hold values from 0.1 to 1.9
- out_weight: bfloat16 [4096, 4096], P('tp', 'kv'), may hold values from -0.09375 to 0.09375
- last_norm_gain: float32 [4096], P(('kv', 'tp')), may hold values from 0.1 to 1.9
- second_gate: bfloat16 [4096, 11264], P('kv', 'tp'), may hold values from -0.09375 to 0.09375
- second_up: bfloat16 [4096, 11264], P('kv', 'tp'), may hold values from -0.09375 to 0.09375
- second_down: bfloat16 [11264, 4096], P('tp', 'kv'), may hold values from -0.109375 to 0.109375
Outputs:
- next_stream: bfloat16 [128, 4096], P(None, ('kv', 'tp'))
- ssm_next: float32 [128, 64, 64, 128], P('kv', 'tp')
- conv_next: bfloat16 [128, 3, 8, 768], P('kv', None, 'tp')
All inputs are finite; a program needn't handle non-finite values.
Results may differ from a plain program's by a relative error of at most 0.015.
Values may be sent and summed in bfloat16 or wider, within the bound.
A program may use at most 128 MiB of HBM per device.

v0:
```python
import jax
import jax.numpy as jnp
from jax import lax
from jax.sharding import PartitionSpec as P

norm_epsilon = 1e-06


def row_factor(total_squares, width):
    return lax.rsqrt(total_squares / width + norm_epsilon)[:, None]


def normed_rows(stream, gain):
    values = stream.astype(jnp.float32)
    scaled = (values * gain[None]).astype(jnp.bfloat16)
    squares = jnp.sum(values * values, axis=1)
    gathered, square_cols = (
        lax.all_gather(scaled, "tp", axis=1, tiled=True),
        lax.all_gather(squares[:, None].astype(jnp.bfloat16), "tp", axis=1, tiled=True).astype(
            jnp.float32
        ),
    )
    return (gathered, jnp.sum(square_cols, axis=1))


def finish(stream, terms, weight_matrix):
    branch_output = lax.psum_scatter(
        terms.astype(jnp.bfloat16), "tp", scatter_dimension=1, tiled=True
    ).astype(jnp.float32)
    return (stream.astype(jnp.float32) + weight_matrix * branch_output).astype(jnp.bfloat16)


def channel_mixer(stream, gain, gate_weight, up_weight, down_weight):
    width = stream.shape[1] * lax.axis_size("kv") * lax.axis_size("tp")
    gathered, squares = normed_rows(stream, gain)
    gate_part = jnp.dot(gathered, gate_weight, preferred_element_type=jnp.float32)
    up_part = jnp.dot(gathered, up_weight, preferred_element_type=jnp.float32)
    gate_sum, up_sum, total = lax.psum((gate_part, up_part, squares), "kv")
    factor = row_factor(total, width)
    hidden = (jax.nn.silu(gate_sum * factor) * (up_sum * factor)).astype(jnp.bfloat16)
    terms = jnp.dot(hidden, down_weight, preferred_element_type=jnp.float32)
    return finish(stream, terms, 0.5)


def token_mixer(
    stream,
    ssm_state,
    conv_state,
    gain,
    gate_in,
    value_in,
    write_in,
    read_in,
    step_in,
    conv_weight,
    step_bias,
    log_decay_rate,
    group_gain,
    out_weight,
):
    width_all = stream.shape[1] * lax.axis_size("kv") * lax.axis_size("tp")
    gathered, squares = normed_rows(stream, gain)
    gate_part = jnp.dot(gathered, gate_in, preferred_element_type=jnp.float32)
    value_part = jnp.dot(gathered, value_in, preferred_element_type=jnp.float32)
    write_part = jnp.dot(gathered, write_in, preferred_element_type=jnp.float32)
    read_part = jnp.dot(gathered, read_in, preferred_element_type=jnp.float32)
    step_part = jnp.dot(gathered, step_in, preferred_element_type=jnp.float32)
    count = stream.shape[0] // lax.axis_size("kv")
    gate_sum, value_sum, write_sum, read_sum, step_sum, total = (
        lax.psum_scatter(gate_part, "kv", scatter_dimension=0, tiled=True),
        lax.psum_scatter(value_part, "kv", scatter_dimension=0, tiled=True),
        lax.psum_scatter(write_part, "kv", scatter_dimension=0, tiled=True),
        lax.psum_scatter(read_part, "kv", scatter_dimension=0, tiled=True),
        lax.psum_scatter(step_part, "kv", scatter_dimension=0, tiled=True),
        lax.psum_scatter(squares, "kv", scatter_dimension=0, tiled=True),
    )
    factor = row_factor(total, width_all)
    gate = (gate_sum * factor).astype(jnp.bfloat16)
    values = (value_sum * factor).astype(jnp.bfloat16)
    writes = (write_sum * factor).astype(jnp.bfloat16)
    reads = (read_sum * factor).astype(jnp.bfloat16)
    steps = (step_sum * factor).astype(jnp.bfloat16)
    groups = conv_weight.shape[1]
    state_size = write_in.shape[1] // groups
    heads = step_in.shape[1]
    head_size = value_in.shape[1] // heads
    per_group = heads // groups
    width = per_group * head_size
    fresh = jnp.concatenate(
        [
            values.reshape(count, groups, width),
            writes.reshape(count, groups, state_size),
            reads.reshape(count, groups, state_size),
        ],
        axis=2,
    )
    window = jnp.concatenate([conv_state, fresh[:, None]], axis=1)
    activated = jax.nn.silu(jnp.sum(window.astype(jnp.float32) * conv_weight[None], axis=1))
    inputs = activated[:, :, :width].reshape(count, groups, per_group, head_size)
    write_vec = activated[:, :, width : width + state_size]
    read_vec = activated[:, :, width + state_size :]
    step_size = jax.nn.softplus(steps.astype(jnp.float32) + step_bias[None])
    decay = jnp.exp(-step_size * jnp.exp(log_decay_rate)[None])
    step_size = step_size.reshape(count, groups, per_group)
    decay = decay.reshape(count, groups, per_group)
    carried = ssm_state.reshape(count, groups, per_group, head_size, state_size)
    updated = (
        carried * decay[:, :, :, None, None]
        + (step_size[:, :, :, None] * inputs)[..., None] * write_vec[:, :, None, None, :]
    )
    readout = jnp.einsum("bghpn,bgn->bghp", updated, read_vec).reshape(count, groups, width)
    gated = readout * jax.nn.silu(gate.astype(jnp.float32)).reshape(count, groups, width)
    normed = gated * lax.rsqrt(jnp.mean(gated * gated, axis=2, keepdims=True) + norm_epsilon)
    mixed = (
        (normed * group_gain.reshape(groups, width)[None])
        .astype(jnp.bfloat16)
        .reshape(count, groups * width)
    )
    terms = jnp.dot(
        lax.all_gather(mixed, "kv", axis=0, tiled=True),
        out_weight,
        preferred_element_type=jnp.float32,
    )
    after = finish(stream, terms, 1.0)
    return (after, updated.reshape(ssm_state.shape), window[:, 1:])


def on_device(
    stream,
    ssm_state,
    conv_state,
    first_gain,
    first_gate,
    first_up,
    first_down,
    mix_gain,
    gate_in,
    value_in,
    write_in,
    read_in,
    step_in,
    conv_weight,
    step_bias,
    log_decay_rate,
    group_gain,
    out_weight,
    last_norm_gain,
    second_gate,
    second_up,
    second_down,
):
    after_first = channel_mixer(stream, first_gain, first_gate, first_up, first_down)
    after_mix, ssm_next, conv_next = token_mixer(
        after_first,
        ssm_state,
        conv_state,
        mix_gain,
        gate_in,
        value_in,
        write_in,
        read_in,
        step_in,
        conv_weight,
        step_bias,
        log_decay_rate,
        group_gain,
        out_weight,
    )
    next_stream = channel_mixer(after_mix, last_norm_gain, second_gate, second_up, second_down)
    return (next_stream, ssm_next, conv_next)


def solution(mesh):
    return jax.shard_map(
        on_device,
        mesh=mesh,
        in_specs=(
            P(None, ("kv", "tp")),
            P("kv", "tp", None, None),
            P("kv", None, "tp", None),
            P(("kv", "tp")),
            P("kv", "tp"),
            P("kv", "tp"),
            P("tp", "kv"),
            P(("kv", "tp")),
            P("kv", "tp"),
            P("kv", "tp"),
            P("kv", "tp"),
            P("kv", "tp"),
            P("kv", "tp"),
            P(None, "tp", None),
            P("tp"),
            P("tp"),
            P("tp"),
            P("tp", "kv"),
            P(("kv", "tp")),
            P("kv", "tp"),
            P("kv", "tp"),
            P("tp", "kv"),
        ),
        out_specs=(P(None, ("kv", "tp")), P("kv", "tp", None, None), P("kv", None, "tp", None)),
        check_vma=False,
    )
```

profile of v0, /device:TPU:27, one launch (start us, length us, event | category | flops | bytes accessed | tf_op | source)
XLA Modules:
  0.0 723.0 jit_solution(3051785513873961415)
XLA Ops:
  7.2 1.0 fusion.14
  8.3 6.1 all_gather.21
  14.3 1.7 fusion.29
  16.0 1.7 fusion.28
  17.7 5.1 all-gather
  22.8 14.4 %psum.43 = f32[128]{0:T(128)S(1)} all-reduce(f32[128]{0:T(128)S(1)} %convert_reduce_fusion.2), channel_id=1, replica_groups=mesh['kv'=8,'tp'=4] {'kv'}, use_global_device_ids=true, to_apply=%region_3.0 | all-reduce | flops 128 | bytes 1024 | tf_op jit(solution)/shard_map/psum | solution.py:38
  37.3 102.2 %all-reduce.8.cloned.1.call-done = (f32[128,2816]{1,0:T(8,128)}, f32[128,2816]{1,0:T(8,128)}) async-done(((f32[128,2816]{1,0:T(8,128)}, f32[128,2816]{1,0:T(8,128)}), (f32[128,2816]{1,0:T(8,128)}, f32[128,2816]{1,0:T(8,128)})) %all-reduce.8.cloned.1.call-update) | async-done | bytes 2883600 | tf_op jit(solution)/shard_map/psum | solution.py:38
  139.4 3.4 convolution_convert_fusion.2
  142.9 0.8 copy.35
  143.7 20.1 %reduce-scatter.25.cloned.1.call-done = bf16[128,128]{1,0:T(8,128)(2,1)} async-done(((bf16[512,128]{1,0:T(8,128)(2,1)}), bf16[128,128]{1,0:T(8,128)(2,1)}) %reduce-scatter.25.cloned.1.call-update) | async-done | bytes 32784
  163.9 0.9 copy.36
  164.7 0.1 fusion.17
  164.9 6.5 all_gather.23
  171.4 0.8 fusion.30
  172.3 0.8 fusion.32
  173.2 1.8 fusion.33
  175.1 2.3 fusion.34
  177.5 2.3 fusion.31
  180.0 0.6 dynamic-slice
  181.2 5.1 all-gather.1
  186.3 13.4 %all-reduce = f32[128]{0:T(128)S(1)} all-reduce(f32[128]{0:T(128)S(1)} %convert_reduce_fusion.1), channel_id=4, replica_groups=mesh['kv'=8,'tp'=4] {'kv'}, use_global_device_ids=true, to_apply=%region_9.10.clone | all-reduce | flops 128 | bytes 1024
  199.7 0.1 fusion.23
  199.8 30.6 %reduce-scatter.15.cloned.1.call-done = f32[16,16]{1,0:T(8,128)} async-done(((f32[128,16]{1,0:T(8,128)}), f32[16,16]{1,0:T(8,128)}) %reduce-scatter.15.cloned.1.call-update) | async-done | bytes 1040 | tf_op jit(solution)/shard_map/reduce_scatter | solution.py:74
  230.4 0.8 multiply_exponential_fusion
  231.2 0.1 copy.31
  231.3 0.7 copy.32
  232.1 0.1 copy.30
  232.1 63.1 %reduce-scatter.19.cloned.1.call-done = f32[16,256]{1,0:T(8,128)} async-done(((f32[128,256]{1,0:T(8,128)}), f32[16,256]{1,0:T(8,128)}) %reduce-scatter.19.cloned.1.call-update) | async-done | bytes 16400 | tf_op jit(solution)/shard_map/reduce_scatter | solution.py:72
  295.2 64.1 %reduce-scatter.21.cloned.1.call-done = f32[16,256]{1,0:T(8,128)} async-done(((f32[128,256]{1,0:T(8,128)}), f32[16,256]{1,0:T(8,128)}) %reduce-scatter.21.cloned.1.call-update) | async-done | bytes 16400 | tf_op jit(solution)/shard_map/reduce_scatter | solution.py:73
  359.4 0.8 multiply_convert_fusion.8
  360.2 64.8 %reduce-scatter.23.cloned.1.call-done = f32[16,1024]{1,0:T(8,128)} async-done(((f32[128,1024]{1,0:T(8,128)}), f32[16,1024]{1,0:T(8,128)}) %reduce-scatter.23.cloned.1.call-update) | async-done | bytes 65552 | tf_op jit(solution)/shard_map/reduce_scatter | solution.py:70
  425.0 65.4 %reduce-scatter.17.cloned.1.call-done = f32[16,1024]{1,0:T(8,128)} async-done(((f32[128,1024]{1,0:T(8,128)}), f32[16,1024]{1,0:T(8,128)}) %reduce-scatter.17.cloned.1.call-update) | async-done | bytes 65552 | tf_op jit(solution)/shard_map/reduce_scatter | solution.py:71
  490.4 1.0 convert_multiply_fusion.6
  491.5 0.3 multiply_reduce_fusion
  491.8 0.1 divide_multiply_fusion
  492.0 0.1 reshape.101
  492.1 0.1 reshape.103
  492.2 0.8 broadcast_multiply_fusion.1
  493.0 5.8 fusion
  498.8 0.7 reshape.102
  499.6 0.1 multiply_reduce_fusion.1
  499.7 0.1 mul.267
  499.8 0.9 multiply_convert_fusion.4
  500.7 24.7 %all_gather.25 = bf16[128,1024]{1,0:T(8,128)(2,1)S(1)} all-gather(bf16[16,1024]{1,0:T(8,128)(2,1)S(1)} %multiply_convert_fusion.4), channel_id=1, replica_groups=mesh['kv'=8,'tp'=4] {'kv'}, dimensions={0}, use_global_device_ids=true | all-gather | bytes 294912 | tf_op jit(solution)/shard_map/all_gather | solution.py:120
  525.4 1.5 convolution_convert_fusion
  527.0 0.8 copy.37
  527.8 27.8 %reduce-scatter.27.cloned.1.call-done = bf16[128,128]{1,0:T(8,128)(2,1)} async-done(((bf16[512,128]{1,0:T(8,128)(2,1)}), bf16[128,128]{1,0:T(8,128)(2,1)}) %reduce-scatter.27.cloned.1.call-update) | async-done | bytes 32784
  555.6 0.9 copy.38
  556.4 1.4 fusion.20
  557.9 6.5 all_gather.26
  564.4 3.5 fusion.36
  567.8 1.7 fusion.35
  569.6 0.1 reshape.104
  569.7 0.8 broadcast_multiply_fusion
  570.5 5.2 all-gather.2
  575.7 14.4 %psum.46 = f32[128]{0:T(128)S(1)} all-reduce(f32[128]{0:T(128)S(1)} %convert_reduce_fusion), channel_id=1, replica_groups=mesh['kv'=8,'tp'=4] {'kv'}, use_global_device_ids=true, to_apply=%region_20.21 | all-reduce | flops 128 | bytes 1024 | tf_op jit(solution)/shard_map/psum | solution.py:38
  590.1 100.2 %all-reduce.6.cloned.1.call-done = (f32[128,2816]{1,0:T(8,128)}, f32[128,2816]{1,0:T(8,128)}) async-done(((f32[128,2816]{1,0:T(8,128)}, f32[128,2816]{1,0:T(8,128)}), (f32[128,2816]{1,0:T(8,128)}, f32[128,2816]{1,0:T(8,128)})) %all-reduce.6.cloned.1.call-update) | async-done | bytes 2883600 | tf_op jit(solution)/shard_map/psum | solution.py:38
  690.3 3.4 convolution_convert_fusion.1
  693.7 0.7 copy.39
  694.5 8.4 %multiply_add_fusion = f32[16,16,64,128]{3,2,1,0:T(8,128)} fusion(f32[16,16,64,128]{3,2,1,0:T(8,128)} %param.23, f32[16,16,128]{2,1,0:T(8,128)S(1)} %broadcast_bitcast_fusion, f32[16,16,64]{2,1,0:T(8,128)S(1)} %broadcast_multiply_fusion, f32[16,16]{1,0:T(8,128)S(1)} %copy-done.7), kind=kLoop, calls=%fused_computation | loop fusion | flops 6291456 | bytes 16974848 | tf_op jit(solution)/shard_map/add | solution.py:108
  702.9 0.9 fusion.9
  703.7 11.0 %reduce-scatter.29.cloned.1.call-done = bf16[128,128]{1,0:T(8,128)(2,1)} async-done(((bf16[512,128]{1,0:T(8,128)(2,1)}), bf16[128,128]{1,0:T(8,128)(2,1)}) %reduce-scatter.29.cloned.1.call-update) | async-done | bytes 32784
  714.7 0.9 copy.40
  715.5 0.6 fusion.21
  (67 shorter events, 1.0 us)
Async XLA Ops:
  7.2 7.2 copy-start
  7.2 132.3 %all-reduce.8.cloned.1.call-start = ((), (), s32[]{:S(2)}) async-start(), calls=%async_computation.17 | async-start | bytes 5767168 | tf_op jit(solution)/shard_map/psum | solution.py:38
  7.2 8.8 %copy-start.1 = (bf16[512,2816]{1,0:T(8,128)(2,1)S(1)}, bf16[512,2816]{1,0:T(8,128)(2,1)}, u32[]{:S(2)}) copy-start(bf16[512,2816]{1,0:T(8,128)(2,1)} %param.26) | copy-start | bytes 8650756
  17.7 146.2 %reduce-scatter.25.cloned.1.call-start = ((), (), s32[]{:S(2)}) async-start(), calls=%async_computation.13 | async-start | bytes 163840
  139.4 25.3 %copy-start.5 = (bf16[128,128]{1,0:T(8,128)(2,1)S(1)}, bf16[128,128]{1,0:T(8,128)(2,1)}, u32[]{:S(2)}) copy-start(bf16[128,128]{1,0:T(8,128)(2,1)} %param.22) | copy-start | bytes 98308
  139.4 25.4 %copy-start.11 = (f32[128]{0:T(128)S(1)}, f32[128]{0:T(128)}, u32[]{:S(2)}) copy-start(f32[128]{0:T(128)} %param.29) | copy-start | bytes 1540
  139.4 32.0 %copy-start.10 = (bf16[512,16]{0,1:T(8,128)(2,1)S(1)}, bf16[512,16]{0,1:T(8,128)(2,1)}, u32[]{:S(2)}) copy-start(bf16[512,16]{0,1:T(8,128)(2,1)} %param.34) | copy-start | bytes 49156
  139.4 32.9 %copy-start.4 = (bf16[512,256]{1,0:T(8,128)(2,1)S(1)}, bf16[512,256]{1,0:T(8,128)(2,1)}, u32[]{:S(2)}) copy-start(bf16[512,256]{1,0:T(8,128)(2,1)} %param.32) | copy-start | bytes 786436
  143.7 86.7 %reduce-scatter.15.cloned.1.call-start = ((), (), s32[]{:S(2)}) async-start(), calls=%async_computation.8 | async-start | bytes 73728 | tf_op jit(solution)/shard_map/reduce_scatter | solution.py:74
  172.2 7.7 %copy-start.13 = (f32[16]{0:T(128)S(1)}, f32[16]{0:T(128)}, u32[]{:S(2)}) copy-start(f32[16]{0:T(128)} %param.37) | copy-start | bytes 196
  172.2 7.8 %copy-start.14 = (u32[32]{0:T(128)S(1)}, u32[32]{0:T(128)}, u32[]{:S(2)}) copy-start(u32[32]{0:T(128)} %constant.31) | copy-start | bytes 388
  172.2 58.2 %copy-start.12 = (f32[16]{0:T(128)S(1)}, f32[16]{0:T(128)}, u32[]{:S(2)}) copy-start(f32[16]{0:T(128)} %param.36) | copy-start | bytes 196
  172.2 123.0 %reduce-scatter.19.cloned.1.call-start = ((), (), s32[]{:S(2)}) async-start(), calls=%async_computation.10 | async-start | bytes 147456 | tf_op jit(solution)/shard_map/reduce_scatter | solution.py:72
  173.2 318.3 %copy-start.3 = (bf16[16,3,2,768]{3,2,1,0:T(2,128)(2,1)S(1)}, bf16[16,3,2,768]{3,2,1,0:T(2,128)(2,1)}, u32[]{:S(2)}) copy-start(bf16[16,3,2,768]{3,2,1,0:T(2,128)(2,1)} %param.24) | copy-start | bytes 442372
  173.2 318.3 %copy-start.9 = (f32[4,2,768]{2,1,0:T(2,128)S(1)}, f32[4,2,768]{2,1,0:T(2,128)}, u32[]{:S(2)}) copy-start(f32[4,2,768]{2,1,0:T(2,128)} %param.35) | copy-start | bytes 73732
  173.2 186.2 %reduce-scatter.21.cloned.1.call-start = ((), (), s32[]{:S(2)}) async-start(), calls=%async_computation.11 | async-start | bytes 147456 | tf_op jit(solution)/shard_map/reduce_scatter | solution.py:73
  175.1 249.9 %reduce-scatter.23.cloned.1.call-start = ((), (), s32[]{:S(2)}) async-start(), calls=%async_computation.12 | async-start | bytes 589824 | tf_op jit(solution)/shard_map/reduce_scatter | solution.py:70
  177.5 312.9 %reduce-scatter.17.cloned.1.call-start = ((), (), s32[]{:S(2)}) async-start(), calls=%async_computation.9 | async-start | bytes 589824 | tf_op jit(solution)/shard_map/reduce_scatter | solution.py:71
  179.9 375.7 %reduce-scatter.27.cloned.1.call-start = ((), (), s32[]{:S(2)}) async-start(), calls=%async_computation.14 | async-start | bytes 163840
  231.2 260.7 %copy-start.6 = (f32[16,16]{1,0:T(8,128)}, f32[16,16]{1,0:T(8,128)S(1)}, u32[]{:S(2)}) copy-start(f32[16,16]{1,0:T(8,128)S(1)} %get-tuple-element.7) | copy-start | bytes 3076
  231.2 260.7 %copy-start.8 = (f32[16,16]{1,0:T(8,128)}, f32[16,16]{1,0:T(8,128)S(1)}, u32[]{:S(2)}) copy-start(f32[16,16]{1,0:T(8,128)S(1)} %get-tuple-element.8) | copy-start | bytes 3076
  527.8 162.5 %all-reduce.6.cloned.1.call-start = ((), (), s32[]{:S(2)}) async-start(), calls=%async_computation.16 | async-start | bytes 5767168 | tf_op jit(solution)/shard_map/psum | solution.py:38
  556.4 11.4 %copy-start.2 = (bf16[512,2816]{1,0:T(8,128)(2,1)S(1)}, bf16[512,2816]{1,0:T(8,128)(2,1)}, u32[]{:S(2)}) copy-start(bf16[512,2816]{1,0:T(8,128)(2,1)} %param.41) | copy-start | bytes 8650756
  569.5 145.2 %reduce-scatter.29.cloned.1.call-start = ((), (), s32[]{:S(2)}) async-start(), calls=%async_computation.15 | async-start | bytes 163840
  690.3 4.2 copy-start.7
Sparse Core Ops, SparseCore 0:
  17.8 121.5 all-reduce.7
  143.8 20.0 reduce-scatter.24
  172.3 58.0 reduce-scatter.14
  234.2 61.0 reduce-scatter.18
  298.4 60.9 reduce-scatter.20
  363.1 61.8 reduce-scatter.22
  428.4 62.0 reduce-scatter.16
  527.9 27.6 reduce-scatter.26
  569.6 120.5 all-reduce.5
  694.6 20.0 reduce-scatter.28
where the time goes:
time: 726 us; the launch traced here: 723 us
  waiting for transfers between devices  549 us (76%)
  blocking collectives  101 us (14%)
  matrix products  30.7 us (4%)
  other arithmetic  18.2 us (3%)
  between operations  15.2 us (2%)
  local copies, waits for them, and re-layouts  7.67 us (1%)
    psum x2, waiting for transfers between devices, channel_mixer(): gate_sum, up_sum, total = lax.psum((gate_part, up_part, squares), 'kv')  202 us
    reduce_scatter x1, waiting for transfers between devices, token_mixer(): lax.psum_scatter(value_part, 'kv', scatter_dimension=0, tiled=True)  65.4 us
    reduce_scatter x1, waiting for transfers between devices, token_mixer(): lax.psum_scatter(gate_part, 'kv', scatter_dimension=0, tiled=True)  64.8 us
    reduce_scatter x1, waiting for transfers between devices, token_mixer(): lax.psum_scatter(read_part, 'kv', scatter_dimension=0, tiled=True)  64.1 us
    reduce_scatter x1, waiting for transfers between devices, token_mixer(): lax.psum_scatter(write_part, 'kv', scatter_dimension=0, tiled=True)  63.1 us
    unnamed x13, waiting for transfers between devices  59 us
    reduce_scatter x1, waiting for transfers between devices, token_mixer(): lax.psum_scatter(step_part, 'kv', scatter_dimension=0, tiled=True)  30.6 us
    psum x2, blocking collectives, channel_mixer(): gate_sum, up_sum, total = lax.psum((gate_part, up_part, squares), 'kv')  28.8 us
  transfers between devices with their start and end apart: 10, of which 10 were waited for; matrix products, arithmetic and copies ran while one was open for 3% of the time, Pallas kernels for 0%

commit v1 on v0

v1 whole, which is shorter than its diff:
```python
import functools

import jax
import jax.numpy as jnp
from jax import lax
from jax.experimental import pallas as pl
from jax.experimental.pallas import tpu as pltpu
from jax.sharding import PartitionSpec as P

norm_epsilon = 1e-06
MESH = pl.DeviceIdType.MESH
LANES = 128
VM = pl.BlockSpec(memory_space=pltpu.VMEM)


def row_factor(total_squares, width):
    return lax.rsqrt(total_squares / width + norm_epsilon)[:, None]


def barrier(axis, n):
    me = lax.axis_index(axis)
    sem = pltpu.get_barrier_semaphore()
    for d in range(1, n):
        pl.semaphore_signal(sem, inc=1, device_id={axis: lax.rem(me + d, n)}, device_id_type=MESH)
    pl.semaphore_wait(sem, n - 1)


def remote(axis, peer, source, target, send, recv):
    return pltpu.make_async_remote_copy(
        src_ref=source,
        dst_ref=target,
        send_sem=send,
        recv_sem=recv,
        device_id={axis: peer},
        device_id_type=MESH,
    )


def block(ref, k, width, split):
    if split:
        return ref.at[k]
    return ref.at[:, pl.ds(pl.multiple_of(k * width, LANES), width)]


def scatter_start(axis, n, source_of, slots, send, recv):
    me = lax.axis_index(axis)
    copies = []
    for d in range(1, n):
        peer = lax.rem(me + d, n)
        copy = remote(axis, peer, source_of(peer), slots.at[d - 1], send.at[d - 1], recv.at[d - 1])
        copy.start()
        copies.append(copy)
    return copies


def gather(axis, n, target_of, send, recv):
    me = lax.axis_index(axis)
    copies = []
    for d in range(1, n):
        peer = lax.rem(me + d, n)
        copy = remote(axis, peer, target_of(me), target_of(me), send.at[d - 1], recv.at[d - 1])
        copy.start()
        copies.append(copy)
    for d in range(1, n):
        left = lax.rem(me - d + n, n)
        remote(axis, left, target_of(left), target_of(left), send.at[d - 1], recv.at[d - 1]).wait_recv()
    return copies


def call(kernel, outs, scratch, ident, *operands):
    return pl.pallas_call(
        kernel,
        out_shape=outs,
        in_specs=[VM] * len(operands),
        out_specs=jax.tree.map(lambda _: VM, outs),
        scratch_shapes=scratch,
        compiler_params=pltpu.CompilerParams(
            collective_id=ident, has_side_effects=True, vmem_limit_bytes=24 * 1024 * 1024
        ),
    )(*operands)


def sems(n):
    return pltpu.SemaphoreType.DMA((n - 1,))


def features_shape(rows, width, n, split):
    return (n, rows, width) if split else (rows, n * width)


def first_gather_kernel(n, split, stream_ref, gains_ref, out_ref, gains_out, s0, r0, s1, r1):
    width = stream_ref.shape[1]
    me = lax.axis_index("tp")
    if split:
        out_ref[me] = stream_ref[...]
    else:
        out_ref[:, pl.ds(pl.multiple_of(me * width, LANES), width)] = stream_ref[...]
    gains_out[me] = gains_ref[...]
    barrier("tp", n)
    copies = gather("tp", n, lambda k: block(out_ref, k, width, split), s0, r0)
    copies += gather("tp", n, lambda k: gains_out.at[k], s1, r1)
    for copy in copies:
        copy.wait_send()


def finish_kernel(n, split, weight, last, terms_ref, stream_ref, *refs):
    if last:
        after_ref, slots, s0, r0 = refs
    else:
        after_ref, out_ref, slots, s0, r0, s1, r1 = refs
    width = stream_ref.shape[1]
    me = lax.axis_index("tp")
    barrier("tp", n)
    copies = scatter_start("tp", n, lambda k: block(terms_ref, k, width, split), slots, s0, r0)
    if split:
        total = terms_ref[me].astype(jnp.float32)
    else:
        total = terms_ref[:, pl.ds(pl.multiple_of(me * width, LANES), width)].astype(jnp.float32)
    for d in range(1, n):
        copies[d - 1].wait_recv()
        total = total + slots[d - 1].astype(jnp.float32)
    after = (stream_ref[...].astype(jnp.float32) + weight * total).astype(jnp.bfloat16)
    after_ref[...] = after
    if not last:
        if split:
            out_ref[me] = after
        else:
            out_ref[:, pl.ds(pl.multiple_of(me * width, LANES), width)] = after
        copies += gather("tp", n, lambda k: block(out_ref, k, width, split), s1, r1)
    for copy in copies:
        copy.wait_send()


def hidden_kernel(n, width, gate_ref, up_ref, side_ref, out_ref, gate_in, up_in, side_in, sg, rg, su, ru, ss, rs, sh, rh):
    me = lax.axis_index("kv")
    barrier("kv", n)
    sides = scatter_start("kv", n, lambda k: side_ref.at[k], side_in, ss, rs)
    gates = scatter_start("kv", n, lambda k: gate_ref.at[k], gate_in, sg, rg)
    ups = scatter_start("kv", n, lambda k: up_ref.at[k], up_in, su, ru)
    for copy in sides + gates + ups:
        copy.wait_recv()
    squares = side_ref[me]
    for d in range(n - 1):
        squares = squares + side_in[d]
    factor = lax.rsqrt(squares / width + norm_epsilon)

    def tile(i, carry):
        cols = pl.ds(pl.multiple_of(i * LANES, LANES), LANES)
        gate = gate_ref[me, :, cols].astype(jnp.float32)
        up = up_ref[me, :, cols].astype(jnp.float32)
        for d in range(n - 1):
            gate = gate + gate_in[d, :, cols].astype(jnp.float32)
            up = up + up_in[d, :, cols].astype(jnp.float32)
        gate = gate * factor
        out_ref[me, :, cols] = (gate / (1.0 + jnp.exp(-gate)) * (up * factor)).astype(jnp.bfloat16)
        return carry

    lax.fori_loop(0, out_ref.shape[2] // LANES, tile, 0)
    copies = gather("kv", n, lambda k: out_ref.at[k], sh, rh)
    for copy in sides + gates + ups + copies:
        copy.wait_send()


def project_kernel(n, count, *refs):
    parts, outs, slots = refs[:count], refs[count : 2 * count], refs[2 * count : 3 * count]
    sem = refs[3 * count :]
    me = lax.axis_index("kv")
    barrier("kv", n)
    copies = []
    for i in range(count):
        copies.append(
            scatter_start("kv", n, lambda k, i=i: parts[i].at[k], slots[i], sem[2 * i], sem[2 * i + 1])
        )
    for i in range(count):
        for copy in copies[i]:
            copy.wait_recv()

        def tile(j, carry, i=i):
            cols = pl.ds(pl.multiple_of(j * LANES, LANES), LANES)
            total = parts[i][me, :, cols].astype(jnp.float32)
            for d in range(n - 1):
                total = total + slots[i][d, :, cols].astype(jnp.float32)
            outs[i][:, cols] = total
            return carry

        lax.fori_loop(0, outs[i].shape[1] // LANES, tile, 0)
    for group in copies:
        for copy in group:
            copy.wait_send()


def rows_gather_kernel(n, rows_ref, out_ref, s0, r0):
    out_ref[lax.axis_index("kv")] = rows_ref[...]
    barrier("kv", n)
    for copy in gather("kv", n, lambda k: out_ref.at[k], s0, r0):
        copy.wait_send()


def is_split(stream):
    return stream.shape[1] % LANES != 0


def joined(gathered, stream):
    if is_split(stream):
        return jnp.swapaxes(gathered, 0, 1).reshape(stream.shape[0], -1)
    return gathered


def normed_rows(features, gain):
    values = features.astype(jnp.float32)
    scaled = (values * gain[None]).astype(jnp.bfloat16)
    return (scaled, jnp.sum(values * values, axis=1))


def finish(stream, terms, weight, ident, last=False):
    n = lax.axis_size("tp")
    rows, width = stream.shape
    split = is_split(stream)
    terms = terms.astype(jnp.bfloat16)
    if split:
        terms = jnp.swapaxes(terms.reshape(rows, n, width), 0, 1)
    outs = [jax.ShapeDtypeStruct((rows, width), jnp.bfloat16)]
    scratch = [pltpu.VMEM((n - 1, rows, width), jnp.bfloat16), sems(n), sems(n)]
    if not last:
        outs.append(jax.ShapeDtypeStruct(features_shape(rows, width, n, split), jnp.bfloat16))
        scratch += [sems(n), sems(n)]
    result = call(
        functools.partial(finish_kernel, n, split, weight, last), outs, scratch, ident, terms, stream
    )
    if last:
        return result[0]
    return (result[0], joined(result[1], stream))


def hidden_units(features, gain, gate_weight, up_weight, ident):
    n = lax.axis_size("kv")
    rows, depth = features.shape
    count, units = rows // n, gate_weight.shape[1]
    scaled, squares = normed_rows(features, gain)
    gate = jnp.dot(scaled, gate_weight, preferred_element_type=jnp.float32).astype(jnp.bfloat16)
    up = jnp.dot(scaled, up_weight, preferred_element_type=jnp.float32).astype(jnp.bfloat16)
    side = jnp.broadcast_to(squares[:, None], (rows, LANES))
    hidden = call(
        functools.partial(hidden_kernel, n, depth * n),
        jax.ShapeDtypeStruct((n, count, units), jnp.bfloat16),
        [
            pltpu.VMEM((n - 1, count, units), jnp.bfloat16),
            pltpu.VMEM((n - 1, count, units), jnp.bfloat16),
            pltpu.VMEM((n - 1, count, LANES), jnp.float32),
        ]
        + [sems(n)] * 8,
        ident,
        gate.reshape(n, count, units),
        up.reshape(n, count, units),
        side.reshape(n, count, LANES),
    )
    return hidden.reshape(rows, units)


def projections(features, gain, gate_in, value_in, write_in, read_in, step_in, ident):
    n = lax.axis_size("kv")
    rows = features.shape[0]
    count = rows // n
    scaled, squares = normed_rows(features, gain)
    parts = [
        jnp.dot(scaled, w, preferred_element_type=jnp.float32).astype(jnp.bfloat16)
        for w in (gate_in, value_in, write_in, read_in)
    ]
    heads = step_in.shape[1]
    step = jnp.dot(scaled, step_in, preferred_element_type=jnp.float32)
    side_width = -(-(heads + 1) // LANES) * LANES
    parts.append(
        jnp.concatenate([step, jnp.broadcast_to(squares[:, None], (rows, side_width - heads))], axis=1)
    )
    parts = [p.reshape(n, count, p.shape[1]) for p in parts]
    sums = call(
        functools.partial(project_kernel, n, len(parts)),
        [jax.ShapeDtypeStruct(p.shape[1:], jnp.float32) for p in parts],
        [pltpu.VMEM((n - 1,) + p.shape[1:], p.dtype) for p in parts] + [sems(n)] * (2 * len(parts)),
        ident,
        *parts,
    )
    return (*sums[:4], sums[4][:, :heads], sums[4][:, heads])


def rows_gather(mixed, ident):
    n = lax.axis_size("kv")
    out = call(
        functools.partial(rows_gather_kernel, n),
        jax.ShapeDtypeStruct((n,) + mixed.shape, mixed.dtype),
        [sems(n), sems(n)],
        ident,
        mixed,
    )
    return out.reshape(n * mixed.shape[0], mixed.shape[1])


def first_gather(stream, gains):
    n = lax.axis_size("tp")
    rows, width = stream.shape
    split = is_split(stream)
    packed = jnp.stack(gains)
    out, packed = call(
        functools.partial(first_gather_kernel, n, split),
        [
            jax.ShapeDtypeStruct(features_shape(rows, width, n, split), stream.dtype),
            jax.ShapeDtypeStruct((n,) + packed.shape, packed.dtype),
        ],
        [sems(n)] * 4,
        0,
        stream,
        packed,
    )
    all_gains = jnp.swapaxes(packed, 0, 1).reshape(len(gains), n * width)
    return (joined(out, stream), all_gains)


def token_mixer(
    features,
    ssm_state,
    conv_state,
    gain,
    gate_in,
    value_in,
    write_in,
    read_in,
    step_in,
    conv_weight,
    step_bias,
    log_decay_rate,
    group_gain,
    out_weight,
):
    width_all = features.shape[1] * lax.axis_size("kv")
    count = features.shape[0] // lax.axis_size("kv")
    gate_sum, value_sum, write_sum, read_sum, step_sum, total = projections(
        features, gain, gate_in, value_in, write_in, read_in, step_in, 3
    )
    factor = row_factor(total, width_all)
    gate = (gate_sum * factor).astype(jnp.bfloat16)
    values = (value_sum * factor).astype(jnp.bfloat16)
    writes = (write_sum * factor).astype(jnp.bfloat16)
    reads = (read_sum * factor).astype(jnp.bfloat16)
    steps = (step_sum * factor).astype(jnp.bfloat16)
    groups = conv_weight.shape[1]
    state_size = write_in.shape[1] // groups
    heads = step_in.shape[1]
    head_size = value_in.shape[1] // heads
    per_group = heads // groups
    width = per_group * head_size
    fresh = jnp.concatenate(
        [
            values.reshape(count, groups, width),
            writes.reshape(count, groups, state_size),
            reads.reshape(count, groups, state_size),
        ],
        axis=2,
    )
    window = jnp.concatenate([conv_state, fresh[:, None]], axis=1)
    activated = jax.nn.silu(jnp.sum(window.astype(jnp.float32) * conv_weight[None], axis=1))
    inputs = activated[:, :, :width].reshape(count, groups, per_group, head_size)
    write_vec = activated[:, :, width : width + state_size]
    read_vec = activated[:, :, width + state_size :]
    step_size = jax.nn.softplus(steps.astype(jnp.float32) + step_bias[None])
    decay = jnp.exp(-step_size * jnp.exp(log_decay_rate)[None])
    step_size = step_size.reshape(count, groups, per_group)
    decay = decay.reshape(count, groups, per_group)
    carried = ssm_state.reshape(count, groups, per_group, head_size, state_size)
    updated = (
        carried * decay[:, :, :, None, None]
        + (step_size[:, :, :, None] * inputs)[..., None] * write_vec[:, :, None, None, :]
    )
    readout = jnp.einsum("bghpn,bgn->bghp", updated, read_vec).reshape(count, groups, width)
    gated = readout * jax.nn.silu(gate.astype(jnp.float32)).reshape(count, groups, width)
    normed = gated * lax.rsqrt(jnp.mean(gated * gated, axis=2, keepdims=True) + norm_epsilon)
    mixed = (
        (normed * group_gain.reshape(groups, width)[None])
        .astype(jnp.bfloat16)
        .reshape(count, groups * width)
    )
    terms = jnp.dot(rows_gather(mixed, 4), out_weight, preferred_element_type=jnp.float32)
    return (terms, updated.reshape(ssm_state.shape), window[:, 1:])


def on_device(
    stream,
    ssm_state,
    conv_state,
    first_gain,
    first_gate,
    first_up,
    first_down,
    mix_gain,
    gate_in,
    value_in,
    write_in,
    read_in,
    step_in,
    conv_weight,
    step_bias,
    log_decay_rate,
    group_gain,
    out_weight,
    last_norm_gain,
    second_gate,
    second_up,
    second_down,
):
    features, gains = first_gather(stream, [first_gain, mix_gain, last_norm_gain])
    hidden = hidden_units(features, gains[0], first_gate, first_up, 1)
    terms = jnp.dot(hidden, first_down, preferred_element_type=jnp.float32)
    after_first, features = finish(stream, terms, 0.5, 2)
    terms, ssm_next, conv_next = token_mixer(
        features,
        ssm_state,
        conv_state,
        gains[1],
        gate_in,
        value_in,
        write_in,
        read_in,
        step_in,
        conv_weight,
        step_bias,
        log_decay_rate,
        group_gain,
        out_weight,
    )
    after_mix, features = finish(after_first, terms, 1.0, 5)
    hidden = hidden_units(features, gains[2], second_gate, second_up, 6)
    terms = jnp.dot(hidden, second_down, preferred_element_type=jnp.float32)
    next_stream = finish(after_mix, terms, 0.5, 7, last=True)
    return (next_stream, ssm_next, conv_next)


def solution(mesh):
    return jax.shard_map(
        on_device,
        mesh=mesh,
        in_specs=(
            P(None, ("kv", "tp")),
            P("kv", "tp", None, None),
            P("kv", None, "tp", None),
            P(("kv", "tp")),
            P("kv", "tp"),
            P("kv", "tp"),
            P("tp", "kv"),
            P(("kv", "tp")),
            P("kv", "tp"),
            P("kv", "tp"),
            P("kv", "tp"),
            P("kv", "tp"),
            P("kv", "tp"),
            P(None, "tp", None),
            P("tp"),
            P("tp"),
            P("tp"),
            P("tp", "kv"),
            P(("kv", "tp")),
            P("kv", "tp"),
            P("kv", "tp"),
            P("tp", "kv"),
        ),
        out_specs=(P(None, ("kv", "tp")), P("kv", "tp", None, None), P("kv", None, "tp", None)),
        check_vma=False,
    )
```

time: 726 us -> 210 us (0.29)
  waiting for transfers between devices: 549 us -> 0 us
  Pallas kernels: 0 us -> 166 us
  blocking collectives: 101 us -> 0 us
  between operations: 15.2 us -> 1.08 us
  matrix products: 30.7 us -> 20.9 us
    reduce_scatter x5 -> x0, waiting for transfers between devices: 288 us -> none  [the longest x1 65.4 us: token_mixer(): lax.psum_scatter(value_part, 'kv', scatter_dimension=0, tiled=True)]
    psum x2 -> x0, waiting for transfers between devices: 202 us -> none  [channel_mixer(): gate_sum, up_sum, total = lax.psum((gate_part, up_part, squares), 'kv')]
    pallas_call x0 -> x8, Pallas kernels: none -> 166 us  [call(): pl.pallas_call(kernel, out_shape=outs, in_specs=[VM] * len(operands), out...]
    all_gather x7 -> x0, blocking collectives: 59.1 us -> none  [the longest x1 24.7 us: token_mixer(): lax.all_gather(mixed, 'kv', axis=0, tiled=True)]
    unnamed x13 -> x0, waiting for transfers between devices: 59 us -> none
    psum x2 -> x0, blocking collectives: 28.8 us -> none  [channel_mixer(): gate_sum, up_sum, total = lax.psum((gate_part, up_part, squares), 'kv')]
    unnamed x1 -> x0, blocking collectives: 13.4 us -> none
    dot_general x12, matrix products: 24.9 us -> 15 us  [the longest x2 4.64 us: hidden_units(): jnp.dot(scaled, gate_weight, preferred_element_type=jnp.float32)]
  transfers between devices with their start and end apart: 10 -> 0, of which waited for: 10 -> 0; matrix products, arithmetic and copies ran while one was open for 3% -> 0% of each run, Pallas kernels for 0% -> 0%
where the time goes in v1:
time: 210 us
  Pallas kernels  166 us (79%)
  matrix products  20.9 us (10%)
  other arithmetic  12.4 us (6%)
  local copies, waits for them, and re-layouts  9.13 us (4%)
    pallas_call x8, Pallas kernels, call(): pl.pallas_call(kernel, out_shape=outs, in_specs=[VM] * len(operands), out...  166 us
    add x1, other arithmetic, token_mixer(): carried * decay[:, :, :, None, None]  8.37 us
    unnamed x40, local copies, waits for them, and re-layouts  6 us
    dot_general x1, matrix products, token_mixer(): jnp.einsum('bghpn,bgn->bghp', updated, read_vec)  5.84 us
    dot_general x2, matrix products, hidden_units(): jnp.dot(scaled, gate_weight, preferred_element_type=jnp.float32)  4.64 us

profile of v1, /device:TPU:27, one launch (start us, length us, event | category | flops | bytes accessed | tf_op | source)
XLA Modules:
  0.0 209.9 jit_solution(9922094337096439224)
XLA Ops:
  0.6 0.0 copy-start
  0.6 0.8 pad_maximum_fusion.1.gains_ref
  1.5 0.8 copy-done.5
  2.3 7.5 %shard_map.229 = (bf16[128,512]{1,0:T(8,128)(2,1)S(1)}, f32[4,3,128]{2,1,0:T(4,128)S(1)}) custom-call(bf16[128,128]{1,0:T(8,128)(2,1)S(1)} %copy-done.5, f32[3,128]{1,0:T(4,128)S(1)} %pad_maximum_fusion.1.gains_ref), custom_call_target="tpu_custom_call" | custom-call | tf_op jit(solution)/shard_map/pallas_call | solution.py:71
  9.9 1.4 convolution_convert_fusion.3
  11.3 1.4 convolution_convert_fusion.2
  12.7 0.1 fusion.8
  12.8 0.1 broadcast_in_dim.12
  12.9 0.1 broadcast_in_dim.13.side_ref
  13.0 0.0 copy-start.1
  13.0 1.1 copy-done.1
  14.1 1.1 copy-done.2
  15.2 54.6 %shard_map.230 = bf16[8,16,2816]{2,1,0:T(8,128)(2,1)S(1)} custom-call(bf16[8,16,2816]{2,1,0:T(8,128)(2,1)S(1)} %bitcast.53, bf16[8,16,2816]{2,1,0:T(8,128)(2,1)S(1)} %bitcast.54, f32[8,16,128]{2,1,0:T(8,128)S(1)} %broadcast_in_dim.13.side_ref), custom_call_target="tpu_custom_call" | custom-call | tf_op jit(solution)/shard_map/pallas_call | solution.py:71
  69.9 0.0 copy-start.12
  69.9 0.0 copy-start.13
  69.9 2.5 %convolution_convert_fusion.8.terms_ref = bf16[128,512]{1,0:T(8,128)(2,1)S(1)} fusion(bf16[128,2816]{1,0:T(8,128)(2,1)S(1)} %bitcast.51, bf16[2816,512]{1,0:T(8,128)(2,1)} %param.28), kind=kOutput, calls=%fused_computation.16 | convolution fusion | flops 369164288 | bytes 3735552 | tf_op jit(solution)/shard_map/dot_general | solution.py:411
  72.4 7.5 %shard_map.231 = (bf16[128,128]{1,0:T(8,128)(2,1)S(1)}, bf16[128,512]{1,0:T(8,128)(2,1)S(1)}) custom-call(bf16[128,512]{1,0:T(8,128)(2,1)S(1)} %convolution_convert_fusion.8.terms_ref, bf16[128,128]{1,0:T(8,128)(2,1)S(1)} %copy-done.6), custom_call_target="tpu_custom_call" | custom-call | tf_op jit(solution)/shard_map/pallas_call | solution.py:71
  80.0 0.3 convolution_convert_fusion.5
  80.3 0.3 convolution_convert_fusion.4
  80.7 0.2 convolution_convert_fusion.10
  80.9 0.2 convolution_convert_fusion.9
  81.1 0.1 fusion.10
  81.2 0.1 broadcast_in_dim.14
  81.2 0.0 copy-done.15
  81.3 0.2 fusion.21
  81.4 0.1 pad_maximum_fusion
  81.5 19.6 %shard_map.232 = (f32[16,1024]{1,0:T(8,128)S(1)}, f32[16,1024]{1,0:T(8,128)S(1)}, f32[16,256]{1,0:T(8,128)S(1)}, f32[16,256]{1,0:T(8,128)S(1)}, f32[16,128]{1,0:T(8,128)S(1)}) custom-call(bf16[8,16,1024]{2,1,0:T(8,128)(2,1)S(1)} %bitcast.58, bf16[8,16,1024]{2,1,0:T(8,128)(2,1)S(1)} %bitcast.59, bf16[8,16,256]{2,1,0:T(8,128)(2,1)S(1)} %bitcast.60, ...), custom_call_target="tpu_custom_call" | custom-call | tf_op jit(solution)/shard_map/pallas_call | solution.py:71
  101.1 0.2 rsqrt_reduce_fusion
  101.3 0.1 multiply_convert_fusion.4
  101.4 0.1 convert_multiply_fusion.6
  101.6 0.3 multiply_reduce_fusion
  101.9 0.1 divide_multiply_fusion
  102.1 0.6 fusion.27
  102.7 0.1 reshape.134
  102.8 0.1 multiply_exponential_fusion
  102.9 0.1 copy.29
  103.0 0.7 copy.30
  103.7 0.8 broadcast_multiply_fusion.1
  104.5 0.1 copy.27
  104.6 0.7 copy.28
  105.3 5.8 %fusion = f32[16,2,1,8,64]{4,2,3,1,0:T(1,128)S(1)} fusion(f32[16,2,128,1,1]{2,3,4,1,0:T(1,128)} %bitcast.74, f32[16,2,8,64,128]{4,3,2,1,0:T(8,128)} %bitcast.64, f32[16,2,128]{2,1,0:T(2,128)S(1)} %get-tuple-element.27, f32[16,2,8,64]{3,2,1,0:T(8,128)S(1)} %broadcast_multiply_fusion.1, f32[16,2,8]{2,1,0:T(2,128)} %copy.28), kind=kOutput, calls=%fused_computation.1 | convolution fusion | flops 10485760 | bytes 8553472 | tf_op jit(solution)/shard_map/bghpn,bgn->bghp/dot_general | solution.py:373
  111.1 0.1 reshape.136
  111.2 0.1 multiply_reduce_fusion.1
  111.4 0.1 mul.225
  111.5 0.1 reshape.135
  111.6 7.5 %shard_map.233 = bf16[8,16,1024]{2,1,0:T(8,128)(2,1)S(1)} custom-call(bf16[16,1024]{1,0:T(8,128)(2,1)S(1)} %multiply_convert_fusion.rows_ref), custom_call_target="tpu_custom_call" | custom-call | tf_op jit(solution)/shard_map/pallas_call | solution.py:71
  119.2 1.5 convolution_convert_fusion.6.terms_ref
  120.7 10.8 %shard_map.234 = (bf16[128,128]{1,0:T(8,128)(2,1)S(1)}, bf16[128,512]{1,0:T(8,128)(2,1)S(1)}) custom-call(bf16[128,512]{1,0:T(8,128)(2,1)S(1)} %convolution_convert_fusion.6.terms_ref, bf16[128,128]{1,0:T(8,128)(2,1)S(1)} %get-tuple-element.22.stream_ref), custom_call_target="tpu_custom_call" | custom-call | tf_op jit(solution)/shard_map/pallas_call | solution.py:71
  131.5 3.2 %convolution_convert_fusion.1 = bf16[128,2816]{1,0:T(8,128)(2,1)} fusion(bf16[512,2816]{1,0:T(8,128)(2,1)} %param.41, bf16[128,512]{1,0:T(8,128)(2,1)S(1)} %get-tuple-element.23, f32[512]{0:T(512)S(1)} %bitcast.77), kind=kOutput, calls=%fused_computation.9 | convolution fusion | flops 369655808 | bytes 3737600 | tf_op jit(solution)/shard_map/dot_general | solution.py:240
  134.8 1.4 convolution_convert_fusion
  136.2 0.1 fusion.12
  136.3 0.1 broadcast_in_dim.16
  136.4 0.1 broadcast_in_dim.17.side_ref
  136.5 0.0 copy-start.3
  136.5 1.1 copy-done.3
  137.6 1.1 copy-done.4
  138.7 53.7 %shard_map.235 = bf16[8,16,2816]{2,1,0:T(8,128)(2,1)S(1)} custom-call(bf16[8,16,2816]{2,1,0:T(8,128)(2,1)S(1)} %bitcast.55, bf16[8,16,2816]{2,1,0:T(8,128)(2,1)S(1)} %bitcast.56, f32[8,16,128]{2,1,0:T(8,128)S(1)} %broadcast_in_dim.17.side_ref), custom_call_target="tpu_custom_call" | custom-call | tf_op jit(solution)/shard_map/pallas_call | solution.py:71
  192.4 2.4 %convolution_convert_fusion.7.terms_ref = bf16[128,512]{1,0:T(8,128)(2,1)S(1)} fusion(bf16[128,2816]{1,0:T(8,128)(2,1)S(1)} %bitcast.52, bf16[2816,512]{1,0:T(8,128)(2,1)} %param.43), kind=kOutput, calls=%fused_computation.15 | convolution fusion | flops 369164288 | bytes 3735552 | tf_op jit(solution)/shard_map/dot_general | solution.py:431
  194.8 5.0 %shard_map.236 = bf16[128,128]{1,0:T(8,128)(2,1)S(1)} custom-call(bf16[128,512]{1,0:T(8,128)(2,1)S(1)} %convolution_convert_fusion.7.terms_ref, bf16[128,128]{1,0:T(8,128)(2,1)S(1)} %get-tuple-element.24.stream_ref), custom_call_target="tpu_custom_call" | custom-call | tf_op jit(solution)/shard_map/pallas_call | solution.py:71
  199.9 0.1 reshape.141
  200.0 0.1 broadcast_multiply_fusion
  200.1 8.4 %multiply_add_fusion = f32[16,16,64,128]{3,2,1,0:T(8,128)} fusion(f32[16,16,64,128]{3,2,1,0:T(8,128)} %param.23, f32[16,16,128]{2,1,0:T(8,128)S(1)} %broadcast_bitcast_fusion, f32[16,16,64]{2,1,0:T(8,128)S(1)} %broadcast_multiply_fusion, f32[16,16]{1,0:T(8,128)S(1)} %get-tuple-element.25), kind=kLoop, calls=%fused_computation | loop fusion | flops 6291456 | bytes 16974848 | tf_op jit(solution)/shard_map/add | solution.py:370
  208.5 0.9 fusion.13
  209.3 0.6 copy.36
  (38 shorter events, 0.2 us)
Async XLA Ops:
  0.6 9.2 %copy-start = (bf16[512,2816]{1,0:T(8,128)(2,1)S(1)}, bf16[512,2816]{1,0:T(8,128)(2,1)}, u32[]{:S(2)}) copy-start(bf16[512,2816]{1,0:T(8,128)(2,1)} %param.26) | copy-start | bytes 8650756
  1.5 0.8 copy-start.5
  2.3 9.0 %copy-start.7 = (bf16[512,2816]{1,0:T(8,128)(2,1)S(1)}, bf16[512,2816]{1,0:T(8,128)(2,1)}, u32[]{:S(2)}) copy-start(bf16[512,2816]{1,0:T(8,128)(2,1)} %param.27) | copy-start | bytes 8650756
  13.0 1.1 copy-start.1
  14.1 1.1 copy-start.2
  15.2 57.1 %copy-start.6 = (bf16[128,128]{1,0:T(8,128)(2,1)S(1)}, bf16[128,128]{1,0:T(8,128)(2,1)}, u32[]{:S(2)}) copy-start(bf16[128,128]{1,0:T(8,128)(2,1)} %stream_ref.3) | copy-start | bytes 98308
  15.2 64.7 %copy-start.9 = (bf16[512,1024]{1,0:T(8,128)(2,1)S(1)}, bf16[512,1024]{1,0:T(8,128)(2,1)}, u32[]{:S(2)}) copy-start(bf16[512,1024]{1,0:T(8,128)(2,1)} %param.30) | copy-start | bytes 3145732
  69.9 10.4 %copy-start.10 = (bf16[512,1024]{1,0:T(8,128)(2,1)S(1)}, bf16[512,1024]{1,0:T(8,128)(2,1)}, u32[]{:S(2)}) copy-start(bf16[512,1024]{1,0:T(8,128)(2,1)} %param.31) | copy-start | bytes 3145732
  69.9 10.8 %copy-start.12 = (bf16[512,256]{1,0:T(8,128)(2,1)S(1)}, bf16[512,256]{1,0:T(8,128)(2,1)}, u32[]{:S(2)}) copy-start(bf16[512,256]{1,0:T(8,128)(2,1)} %param.32) | copy-start | bytes 786436
  69.9 11.0 %copy-start.13 = (bf16[512,256]{1,0:T(8,128)(2,1)S(1)}, bf16[512,256]{1,0:T(8,128)(2,1)}, u32[]{:S(2)}) copy-start(bf16[512,256]{1,0:T(8,128)(2,1)} %param.33) | copy-start | bytes 786436
  72.4 8.9 %copy-start.15 = (bf16[512,16]{0,1:T(8,128)(2,1)S(1)}, bf16[512,16]{0,1:T(8,128)(2,1)}, u32[]{:S(2)}) copy-start(bf16[512,16]{0,1:T(8,128)(2,1)} %param.34) | copy-start | bytes 49156
  72.4 29.2 %copy-start.11 = (bf16[16,3,2,768]{3,2,1,0:T(2,128)(2,1)S(1)}, bf16[16,3,2,768]{3,2,1,0:T(2,128)(2,1)}, u32[]{:S(2)}) copy-start(bf16[16,3,2,768]{3,2,1,0:T(2,128)(2,1)} %param.24) | copy-start | bytes 442372
  72.4 29.2 %copy-start.14 = (f32[4,2,768]{2,1,0:T(2,128)S(1)}, f32[4,2,768]{2,1,0:T(2,128)}, u32[]{:S(2)}) copy-start(f32[4,2,768]{2,1,0:T(2,128)} %param.35) | copy-start | bytes 73732
  80.3 22.5 %copy-start.18 = (f32[16]{0:T(128)S(1)}, f32[16]{0:T(128)}, u32[]{:S(2)}) copy-start(f32[16]{0:T(128)} %param.37) | copy-start | bytes 196
  80.3 22.5 %copy-start.17 = (f32[16]{0:T(128)S(1)}, f32[16]{0:T(128)}, u32[]{:S(2)}) copy-start(f32[16]{0:T(128)} %param.36) | copy-start | bytes 196
  105.3 6.3 %copy-start.16 = (f32[1024]{0:T(1024)S(1)}, f32[1024]{0:T(1024)}, u32[]{:S(2)}) copy-start(f32[1024]{0:T(1024)} %param.38) | copy-start | bytes 12292
  111.6 23.2 %copy-start.8 = (bf16[512,2816]{1,0:T(8,128)(2,1)S(1)}, bf16[512,2816]{1,0:T(8,128)(2,1)}, u32[]{:S(2)}) copy-start(bf16[512,2816]{1,0:T(8,128)(2,1)} %param.42) | copy-start | bytes 8650756
  136.5 1.1 copy-start.3
  137.6 1.1 copy-start.4

commit v2 on v1

--- a/solution.py
+++ b/solution.py
@@ -131,33 +131,84 @@
         copy.wait_send()
 
 
-def hidden_kernel(n, width, gate_ref, up_ref, side_ref, out_ref, gate_in, up_in, side_in, sg, rg, su, ru, ss, rs, sh, rh):
+def hidden_kernel(n, width, gate_ref, up_ref, side_ref, out_ref, side_in, *refs):
+    zn, units = gate_ref.shape[0], gate_ref.shape[3]
+    near, sums, far = refs[0:2], refs[2:4], refs[4:6]
+    ss, rs, sa, ra, sz, rz, sh, rh, sx, rx = refs[6:]
+    parts = (gate_ref, up_ref)
     me = lax.axis_index("kv")
+    z, x = me // 2, lax.rem(me, 2)
+    other = z * 2 + 1 - x
+    tiles = units // LANES
+    cuts = [tiles * i // 4 * LANES for i in range(5)]
+    ranges = [pl.ds(lo, hi - lo) for lo, hi in zip(cuts, cuts[1:])]
     barrier("kv", n)
-    sides = scatter_start("kv", n, lambda k: side_ref.at[k], side_in, ss, rs)
-    gates = scatter_start("kv", n, lambda k: gate_ref.at[k], gate_in, sg, rg)
-    ups = scatter_start("kv", n, lambda k: up_ref.at[k], up_in, su, ru)
-    for copy in sides + gates + ups:
+    sides = scatter_start("kv", n, lambda k: side_ref.at[k // 2, lax.rem(k, 2)], side_in, ss, rs)
+    sent = list(sides)
+    first = {}
+    for c, cols in enumerate(ranges):
+        for i in range(2):
+            copy = remote(
+                "kv", other, parts[i].at[:, 1 - x, :, cols], near[i].at[:, :, cols], sa.at[c, i], ra.at[c, i]
+            )
+            copy.start()
+            first[c, i] = copy
+            sent.append(copy)
+    second = {}
+    for c, cols in enumerate(ranges):
+        for i in range(2):
+            first[c, i].wait_recv()
+            total = parts[i][:, x, :, cols].astype(jnp.float32) + near[i][:, :, cols].astype(jnp.float32)
+            sums[i][:, :, cols] = total.astype(jnp.bfloat16)
+            for d in range(1, zn):
+                zp = lax.rem(z + d, zn)
+                copy = remote(
+                    "kv", zp * 2 + x, sums[i].at[zp, :, cols], far[i].at[d - 1, :, cols],
+                    sz.at[c, i, d - 1], rz.at[c, i, d - 1],
+                )
+                copy.start()
+                second[c, i, d] = copy
+                sent.append(copy)
+    for copy in sides:
         copy.wait_recv()
-    squares = side_ref[me]
+    squares = side_ref[z, x]
     for d in range(n - 1):
         squares = squares + side_in[d]
-    factor = lax.rsqrt(squares / width + norm_epsilon)
-
-    def tile(i, carry):
-        cols = pl.ds(pl.multiple_of(i * LANES, LANES), LANES)
-        gate = gate_ref[me, :, cols].astype(jnp.float32)
-        up = up_ref[me, :, cols].astype(jnp.float32)
-        for d in range(n - 1):
-            gate = gate + gate_in[d, :, cols].astype(jnp.float32)
-            up = up + up_in[d, :, cols].astype(jnp.float32)
-        gate = gate * factor
-        out_ref[me, :, cols] = (gate / (1.0 + jnp.exp(-gate)) * (up * factor)).astype(jnp.bfloat16)
-        return carry
-
-    lax.fori_loop(0, out_ref.shape[2] // LANES, tile, 0)
-    copies = gather("kv", n, lambda k: out_ref.at[k], sh, rh)
-    for copy in sides + gates + ups + copies:
+    factor = lax.rsqrt(squares / width + norm_epsilon)[:, :1]
+
+    def spread(c, d, zq, xq, peer, send, recv):
+        place = out_ref.at[zq, xq, :, ranges[c]]
+        return remote("kv", peer, place, place, send.at[c, d], recv.at[c, d])
+
+    for c, cols in enumerate(ranges):
+        both = []
+        for i in range(2):
+            total = sums[i][z, :, cols].astype(jnp.float32)
+            for d in range(1, zn):
+                second[c, i, d].wait_recv()
+                total = total + far[i][d - 1, :, cols].astype(jnp.float32)
+            both.append(total * factor)
+        gate, up = both
+        out_ref[z, x, :, cols] = (gate / (1.0 + jnp.exp(-gate)) * up).astype(jnp.bfloat16)
+        for d in range(1, zn):
+            copy = spread(c, d - 1, z, x, lax.rem(z + d, zn) * 2 + x, sh, rh)
+            copy.start()
+            sent.append(copy)
+        copy = spread(c, 0, z, x, other, sx, rx)
+        copy.start()
+        sent.append(copy)
+    for c in range(4):
+        for d in range(1, zn):
+            left = lax.rem(z - d + zn, zn)
+            spread(c, d - 1, left, x, left * 2 + x, sh, rh).wait_recv()
+            copy = spread(c, d, left, x, other, sx, rx)
+            copy.start()
+            sent.append(copy)
+    for c in range(4):
+        for d in range(zn):
+            left = lax.rem(z - d + zn, zn)
+            spread(c, d, left, 1 - x, other, sx, rx).wait_recv()
+    for copy in sent:
         copy.wait_send()
 
 
@@ -240,19 +291,23 @@
     gate = jnp.dot(scaled, gate_weight, preferred_element_type=jnp.float32).astype(jnp.bfloat16)
     up = jnp.dot(scaled, up_weight, preferred_element_type=jnp.float32).astype(jnp.bfloat16)
     side = jnp.broadcast_to(squares[:, None], (rows, LANES))
+    zn = n // 2
+    dma = pltpu.SemaphoreType.DMA
     hidden = call(
         functools.partial(hidden_kernel, n, depth * n),
-        jax.ShapeDtypeStruct((n, count, units), jnp.bfloat16),
-        [
-            pltpu.VMEM((n - 1, count, units), jnp.bfloat16),
-            pltpu.VMEM((n - 1, count, units), jnp.bfloat16),
-            pltpu.VMEM((n - 1, count, LANES), jnp.float32),
-        ]
-        + [sems(n)] * 8,
+        jax.ShapeDtypeStruct((zn, 2, count, units), jnp.bfloat16),
+        [pltpu.VMEM((n - 1, count, LANES), jnp.float32)]
+        + [pltpu.VMEM((zn, count, units), jnp.bfloat16)] * 4
+        + [pltpu.VMEM((zn - 1, count, units), jnp.bfloat16)] * 2
+        + [sems(n)] * 2
+        + [dma((4, 2))] * 2
+        + [dma((4, 2, zn - 1))] * 2
+        + [dma((4, zn - 1))] * 2
+        + [dma((4, zn))] * 2,
         ident,
-        gate.reshape(n, count, units),
-        up.reshape(n, count, units),
-        side.reshape(n, count, LANES),
+        gate.reshape(zn, 2, count, units),
+        up.reshape(zn, 2, count, units),
+        side.reshape(zn, 2, count, LANES),
     )
     return hidden.reshape(rows, units)
 

time: 210 us -> 178 us (0.85); the launches traced: 210 us -> 175 us
  Pallas kernels: 166 us -> 131 us
    pallas_call x8, Pallas kernels: 166 us -> 131 us  [call(): pl.pallas_call(kernel, out_shape=outs, in_specs=[VM] * len(operands), out...]
where the time goes in v2:
time: 178 us; the launch traced here: 175 us
  Pallas kernels  131 us (74%)
  matrix products  20.8 us (12%)
  other arithmetic  12.4 us (7%)
  local copies, waits for them, and re-layouts  9.15 us (5%)
    pallas_call x8, Pallas kernels, call(): pl.pallas_call(kernel, out_shape=outs, in_specs=[VM] * len(operands), out...  131 us
    add x1, other arithmetic, token_mixer(): carried * decay[:, :, :, None, None]  8.37 us
    unnamed x40, local copies, waits for them, and re-layouts  6 us
    dot_general x1, matrix products, token_mixer(): jnp.einsum('bghpn,bgn->bghp', updated, read_vec)  5.84 us
    dot_general x2, matrix products, hidden_units(): jnp.dot(scaled, gate_weight, preferred_element_type=jnp.float32)  4.64 us

profile of v2, /device:TPU:27, one launch (start us, length us, event | category | flops | bytes accessed | tf_op | source)
XLA Modules:
  0.0 174.7 jit_solution(17226445133829151300)
XLA Ops:
  0.6 0.0 copy-start
  0.6 0.8 pad_maximum_fusion.1.gains_ref
  1.5 0.8 copy-done.5
  2.3 7.5 %shard_map.229 = (bf16[128,512]{1,0:T(8,128)(2,1)S(1)}, f32[4,3,128]{2,1,0:T(4,128)S(1)}) custom-call(bf16[128,128]{1,0:T(8,128)(2,1)S(1)} %copy-done.5, f32[3,128]{1,0:T(4,128)S(1)} %pad_maximum_fusion.1.gains_ref), custom_call_target="tpu_custom_call" | custom-call | tf_op jit(solution)/shard_map/pallas_call | solution.py:71
  9.9 1.4 convolution_convert_fusion.3
  11.3 1.4 convolution_convert_fusion.2
  12.7 0.1 fusion.8
  12.8 0.1 broadcast_in_dim.12
  12.9 0.1 broadcast_in_dim.13.side_ref
  13.0 0.0 copy-start.1
  13.0 1.1 copy-done.1
  14.1 1.1 copy-done.2
  15.2 35.8 %shard_map.230 = bf16[4,2,16,2816]{3,2,1,0:T(8,128)(2,1)S(1)} custom-call(bf16[4,2,16,2816]{3,2,1,0:T(8,128)(2,1)S(1)} %bitcast.53, bf16[4,2,16,2816]{3,2,1,0:T(8,128)(2,1)S(1)} %bitcast.54, f32[4,2,16,128]{3,2,1,0:T(8,128)S(1)} %broadcast_in_dim.13.side_ref), custom_call_target="tpu_custom_call" | custom-call | tf_op jit(solution)/shard_map/pallas_call | solution.py:71
  51.1 0.0 copy-start.13
  51.1 2.5 %convolution_convert_fusion.8.terms_ref = bf16[128,512]{1,0:T(8,128)(2,1)S(1)} fusion(bf16[128,2816]{1,0:T(8,128)(2,1)S(1)} %bitcast.51, bf16[2816,512]{1,0:T(8,128)(2,1)} %param.28), kind=kOutput, calls=%fused_computation.16 | convolution fusion | flops 369164288 | bytes 3735552 | tf_op jit(solution)/shard_map/dot_general | solution.py:466
  53.6 0.0 copy-start.15
  53.6 8.1 %shard_map.231 = (bf16[128,128]{1,0:T(8,128)(2,1)S(1)}, bf16[128,512]{1,0:T(8,128)(2,1)S(1)}) custom-call(bf16[128,512]{1,0:T(8,128)(2,1)S(1)} %convolution_convert_fusion.8.terms_ref, bf16[128,128]{1,0:T(8,128)(2,1)S(1)} %copy-done.6), custom_call_target="tpu_custom_call" | custom-call | tf_op jit(solution)/shard_map/pallas_call | solution.py:71
  61.8 0.3 convolution_convert_fusion.5
  62.1 0.3 convolution_convert_fusion.4
  62.4 0.2 convolution_convert_fusion.10
  62.6 0.2 convolution_convert_fusion.9
  62.8 0.1 fusion.10
  62.9 0.1 broadcast_in_dim.14
  63.0 0.0 copy-done.15
  63.0 0.2 fusion.21
  63.2 0.1 pad_maximum_fusion
  63.3 20.0 %shard_map.232 = (f32[16,1024]{1,0:T(8,128)S(1)}, f32[16,1024]{1,0:T(8,128)S(1)}, f32[16,256]{1,0:T(8,128)S(1)}, f32[16,256]{1,0:T(8,128)S(1)}, f32[16,128]{1,0:T(8,128)S(1)}) custom-call(bf16[8,16,1024]{2,1,0:T(8,128)(2,1)S(1)} %bitcast.58, bf16[8,16,1024]{2,1,0:T(8,128)(2,1)S(1)} %bitcast.59, bf16[8,16,256]{2,1,0:T(8,128)(2,1)S(1)} %bitcast.60, ...), custom_call_target="tpu_custom_call" | custom-call | tf_op jit(solution)/shard_map/pallas_call | solution.py:71
  83.3 0.2 rsqrt_reduce_fusion
  83.5 0.1 multiply_convert_fusion.4
  83.6 0.1 convert_multiply_fusion.6
  83.8 0.3 multiply_reduce_fusion
  84.1 0.1 divide_multiply_fusion
  84.2 0.6 fusion.27
  84.8 0.1 reshape.134
  85.0 0.1 multiply_exponential_fusion
  85.1 0.1 copy.29
  85.1 0.7 copy.30
  85.8 0.8 broadcast_multiply_fusion.1
  86.6 0.1 copy.27
  86.7 0.7 copy.28
  87.4 5.8 %fusion = f32[16,2,1,8,64]{4,2,3,1,0:T(1,128)S(1)} fusion(f32[16,2,128,1,1]{2,3,4,1,0:T(1,128)} %bitcast.74, f32[16,2,8,64,128]{4,3,2,1,0:T(8,128)} %bitcast.64, f32[16,2,128]{2,1,0:T(2,128)S(1)} %get-tuple-element.27, f32[16,2,8,64]{3,2,1,0:T(8,128)S(1)} %broadcast_multiply_fusion.1, f32[16,2,8]{2,1,0:T(2,128)} %copy.28), kind=kOutput, calls=%fused_computation.1 | convolution fusion | flops 10485760 | bytes 8553472 | tf_op jit(solution)/shard_map/bghpn,bgn->bghp/dot_general | solution.py:428
  93.2 0.1 reshape.136
  93.3 0.1 multiply_reduce_fusion.1
  93.5 0.1 mul.225
  93.6 0.1 reshape.135
  93.7 7.8 %shard_map.233 = bf16[8,16,1024]{2,1,0:T(8,128)(2,1)S(1)} custom-call(bf16[16,1024]{1,0:T(8,128)(2,1)S(1)} %multiply_convert_fusion.rows_ref), custom_call_target="tpu_custom_call" | custom-call | tf_op jit(solution)/shard_map/pallas_call | solution.py:71
  101.6 1.5 convolution_convert_fusion.6.terms_ref
  103.1 10.5 %shard_map.234 = (bf16[128,128]{1,0:T(8,128)(2,1)S(1)}, bf16[128,512]{1,0:T(8,128)(2,1)S(1)}) custom-call(bf16[128,512]{1,0:T(8,128)(2,1)S(1)} %convolution_convert_fusion.6.terms_ref, bf16[128,128]{1,0:T(8,128)(2,1)S(1)} %get-tuple-element.22.stream_ref), custom_call_target="tpu_custom_call" | custom-call | tf_op jit(solution)/shard_map/pallas_call | solution.py:71
  113.7 3.2 %convolution_convert_fusion.1 = bf16[128,2816]{1,0:T(8,128)(2,1)} fusion(bf16[512,2816]{1,0:T(8,128)(2,1)} %param.41, bf16[128,512]{1,0:T(8,128)(2,1)S(1)} %get-tuple-element.23, f32[512]{0:T(512)S(1)} %bitcast.77), kind=kOutput, calls=%fused_computation.9 | convolution fusion | flops 369655808 | bytes 3737600 | tf_op jit(solution)/shard_map/dot_general | solution.py:291
  116.9 1.4 convolution_convert_fusion
  118.3 0.1 fusion.12
  118.4 0.1 broadcast_in_dim.16
  118.5 0.1 broadcast_in_dim.17.side_ref
  118.6 0.0 copy-start.3
  118.6 1.1 copy-done.3
  119.7 1.1 copy-done.4
  120.8 35.9 %shard_map.235 = bf16[4,2,16,2816]{3,2,1,0:T(8,128)(2,1)S(1)} custom-call(bf16[4,2,16,2816]{3,2,1,0:T(8,128)(2,1)S(1)} %bitcast.55, bf16[4,2,16,2816]{3,2,1,0:T(8,128)(2,1)S(1)} %bitcast.56, f32[4,2,16,128]{3,2,1,0:T(8,128)S(1)} %broadcast_in_dim.17.side_ref), custom_call_target="tpu_custom_call" | custom-call | tf_op jit(solution)/shard_map/pallas_call | solution.py:71
  156.7 2.4 %convolution_convert_fusion.7.terms_ref = bf16[128,512]{1,0:T(8,128)(2,1)S(1)} fusion(bf16[128,2816]{1,0:T(8,128)(2,1)S(1)} %bitcast.52, bf16[2816,512]{1,0:T(8,128)(2,1)} %param.43), kind=kOutput, calls=%fused_computation.15 | convolution fusion | flops 369164288 | bytes 3735552 | tf_op jit(solution)/shard_map/dot_general | solution.py:486
  159.1 5.5 %shard_map.236 = bf16[128,128]{1,0:T(8,128)(2,1)S(1)} custom-call(bf16[128,512]{1,0:T(8,128)(2,1)S(1)} %convolution_convert_fusion.7.terms_ref, bf16[128,128]{1,0:T(8,128)(2,1)S(1)} %get-tuple-element.24.stream_ref), custom_call_target="tpu_custom_call" | custom-call | tf_op jit(solution)/shard_map/pallas_call | solution.py:71
  164.6 0.1 reshape.141
  164.7 0.1 broadcast_multiply_fusion
  164.8 8.4 %multiply_add_fusion = f32[16,16,64,128]{3,2,1,0:T(8,128)} fusion(f32[16,16,64,128]{3,2,1,0:T(8,128)} %param.23, f32[16,16,128]{2,1,0:T(8,128)S(1)} %broadcast_bitcast_fusion, f32[16,16,64]{2,1,0:T(8,128)S(1)} %broadcast_multiply_fusion, f32[16,16]{1,0:T(8,128)S(1)} %get-tuple-element.25), kind=kLoop, calls=%fused_computation | loop fusion | flops 6291456 | bytes 16974848 | tf_op jit(solution)/shard_map/add | solution.py:425
  173.2 0.9 fusion.13
  174.1 0.6 copy.36
  (38 shorter events, 0.2 us)
Async XLA Ops:
  0.6 9.2 %copy-start = (bf16[512,2816]{1,0:T(8,128)(2,1)S(1)}, bf16[512,2816]{1,0:T(8,128)(2,1)}, u32[]{:S(2)}) copy-start(bf16[512,2816]{1,0:T(8,128)(2,1)} %param.26) | copy-start | bytes 8650756
  1.5 0.8 copy-start.5
  2.3 9.0 %copy-start.7 = (bf16[512,2816]{1,0:T(8,128)(2,1)S(1)}, bf16[512,2816]{1,0:T(8,128)(2,1)}, u32[]{:S(2)}) copy-start(bf16[512,2816]{1,0:T(8,128)(2,1)} %param.27) | copy-start | bytes 8650756
  13.0 1.1 copy-start.1
  14.1 1.1 copy-start.2
  15.2 38.3 %copy-start.6 = (bf16[128,128]{1,0:T(8,128)(2,1)S(1)}, bf16[128,128]{1,0:T(8,128)(2,1)}, u32[]{:S(2)}) copy-start(bf16[128,128]{1,0:T(8,128)(2,1)} %stream_ref.3) | copy-start | bytes 98308
  15.2 46.5 %copy-start.9 = (bf16[512,1024]{1,0:T(8,128)(2,1)S(1)}, bf16[512,1024]{1,0:T(8,128)(2,1)}, u32[]{:S(2)}) copy-start(bf16[512,1024]{1,0:T(8,128)(2,1)} %param.30) | copy-start | bytes 3145732
  51.1 11.0 %copy-start.10 = (bf16[512,1024]{1,0:T(8,128)(2,1)S(1)}, bf16[512,1024]{1,0:T(8,128)(2,1)}, u32[]{:S(2)}) copy-start(bf16[512,1024]{1,0:T(8,128)(2,1)} %param.31) | copy-start | bytes 3145732
  51.1 11.4 %copy-start.12 = (bf16[512,256]{1,0:T(8,128)(2,1)S(1)}, bf16[512,256]{1,0:T(8,128)(2,1)}, u32[]{:S(2)}) copy-start(bf16[512,256]{1,0:T(8,128)(2,1)} %param.32) | copy-start | bytes 786436
  51.1 11.5 %copy-start.13 = (bf16[512,256]{1,0:T(8,128)(2,1)S(1)}, bf16[512,256]{1,0:T(8,128)(2,1)}, u32[]{:S(2)}) copy-start(bf16[512,256]{1,0:T(8,128)(2,1)} %param.33) | copy-start | bytes 786436
  53.6 9.4 %copy-start.15 = (bf16[512,16]{0,1:T(8,128)(2,1)S(1)}, bf16[512,16]{0,1:T(8,128)(2,1)}, u32[]{:S(2)}) copy-start(bf16[512,16]{0,1:T(8,128)(2,1)} %param.34) | copy-start | bytes 49156
  53.6 30.2 %copy-start.11 = (bf16[16,3,2,768]{3,2,1,0:T(2,128)(2,1)S(1)}, bf16[16,3,2,768]{3,2,1,0:T(2,128)(2,1)}, u32[]{:S(2)}) copy-start(bf16[16,3,2,768]{3,2,1,0:T(2,128)(2,1)} %param.24) | copy-start | bytes 442372
  53.6 30.2 %copy-start.14 = (f32[4,2,768]{2,1,0:T(2,128)S(1)}, f32[4,2,768]{2,1,0:T(2,128)}, u32[]{:S(2)}) copy-start(f32[4,2,768]{2,1,0:T(2,128)} %param.35) | copy-start | bytes 73732
  62.1 22.9 %copy-start.18 = (f32[16]{0:T(128)S(1)}, f32[16]{0:T(128)}, u32[]{:S(2)}) copy-start(f32[16]{0:T(128)} %param.37) | copy-start | bytes 196
  62.1 22.9 %copy-start.17 = (f32[16]{0:T(128)S(1)}, f32[16]{0:T(128)}, u32[]{:S(2)}) copy-start(f32[16]{0:T(128)} %param.36) | copy-start | bytes 196
  87.4 6.3 %copy-start.16 = (f32[1024]{0:T(1024)S(1)}, f32[1024]{0:T(1024)}, u32[]{:S(2)}) copy-start(f32[1024]{0:T(1024)} %param.38) | copy-start | bytes 12292
  93.7 23.2 %copy-start.8 = (bf16[512,2816]{1,0:T(8,128)(2,1)S(1)}, bf16[512,2816]{1,0:T(8,128)(2,1)}, u32[]{:S(2)}) copy-start(bf16[512,2816]{1,0:T(8,128)(2,1)} %param.42) | copy-start | bytes 8650756
  118.6 1.1 copy-start.3
  119.7 1.1 copy-start.4
